TPU v7x, 512 devices: a whole 4x4x16 slice. The times are simulated.
512 devices in a mesh: sp: 64 (over z, y), tp: 8 (over x, core).
Axes of the slice: x: 4, y: 4, z: 16, core: 2. Of those that a mesh axis runs over, the one named last changes fastest.
Arguments:
- stream: bfloat16 [8192, 2048], P(('sp', 'tp')), may hold values from -6 to 6
- wide_head_query: bfloat16 [8192, 1024], P('sp', 'tp'), may hold values from -6 to 6
- broad_attention_lookup_vectors: bfloat16 [8192, 1024], P('sp', 'tp'), may hold values from -6 to 6
- values_wide: bfloat16 [8192, 2048], P('sp', 'tp'), may hold values from -6 to 6
- query_narrow: bfloat16 [8192, 512], P('sp', 'tp'), may hold values from -6 to 6
- keys_narrow: bfloat16 [8192, 512], P('sp', 'tp'), may hold values from -6 to 6
- values_narrow: bfloat16 [8192, 1024], P('sp', 'tp'), may hold values from -6 to 6
- gate_wide: bfloat16 [8192, 2048], P('sp', 'tp'), may hold values from -6 to 6
- gate_narrow: bfloat16 [8192, 1024], P('sp', 'tp'), may hold values from -6 to 6
- log_decay: float32 [2, 8, 8192], P(None, 'tp', 'sp'), may hold values from -1.2 to 0, as said below
- gain_wide: bfloat16 [2048], P('tp'), may hold values from 0.099609375 to 1.8984375
- gain_narrow: bfloat16 [1024], P('tp'), may hold values from 0.099609375 to 1.8984375
- out_wide: bfloat16 [2048, 2048], P('tp'), may hold values from -0.109375 to 0.109375
- out_narrow: bfloat16 [1024, 2048], P('tp'), may hold values from -0.109375 to 0.109375
- gain_mix: bfloat16 [2048], replicated, may hold values from 0.099609375 to 1.8984375
- gain_pre: bfloat16 [2048], replicated, may hold values from 0.099609375 to 1.8984375
- gain_post: bfloat16 [2048], replicated, may hold values from 0.099609375 to 1.8984375
- weight_gate: bfloat16 [2048, 5120], P('sp', 'tp'), may hold values from -0.125 to 0.125
- weight_lin: bfloat16 [2048, 5120], P('sp', 'tp'), may hold values from -0.125 to 0.125
- weight_down: bfloat16 [2048, 5120], P('sp', 'tp'), may hold values from -0.078125 to 0.078125
- taps_gate: bfloat16 [3, 5120], P(None, 'tp'), may hold values from -3 to 3
- taps_lin: bfloat16 [3, 5120], P(None, 'tp'), may hold values from -3 to 3
Outputs:
- stream_out: bfloat16 [8192, 2048], P(('sp', 'tp'))
Inputs may be any that keep to these rules, and one draw needn't show every extreme that they name: `log_decay`: the natural logarithm of the factor by which one head's retained state is multiplied at one position.
All inputs are finite; a program needn't handle non-finite values.
Results may differ from a plain program's by a relative error of at most 0.023.
Values may be sent and summed in bfloat16 or wider, within the bound.
A program may use at most 64 MiB of HBM per device.

v0:
```python
import jax
import jax.numpy as jnp
from jax import lax
from jax.sharding import Mesh
from jax.sharding import PartitionSpec as P

KW = 128
VW = 256
KN = 64
VN = 128
BLOCK = 128
SP = ("sp_0", "sp_1")
SP_TP = ("sp_0", "sp_1", "tp")


EPS = 1e-06
THETA = 10000.0


def sent_together(arrays, axis, dim, along):
    ends, at = ([], 0)
    for a in arrays[:-1]:
        at += a.shape[along]
        ends.append(at)
    both = jnp.concatenate(arrays, axis=along)
    return tuple(jnp.split(lax.all_gather(both, axis, axis=dim, tiled=True), ends, axis=along))


def filled_with(x, identity):
    return jax.tree.map(
        lambda part, zero: jnp.zeros_like(part) + jnp.asarray(zero, part.dtype), x, identity
    )


def collected_together(x, axis):
    leaves = jax.tree.leaves(x)
    sequence = sorted(range(len(leaves)), key=lambda k: -leaves[k].size)
    width = (1, *leaves[sequence[0]].shape)[-1]
    lines = [
        jnp.pad(leaves[k].reshape(-1), (0, -leaves[k].size % width)).reshape(-1, width)
        for k in sequence
    ]
    both, at, found = (lax.all_gather(jnp.concatenate(lines), axis), 0, {})
    for k, line in zip(sequence, lines):
        slab = both[:, at : at + len(line)].reshape(len(both), -1)
        found[k] = slab[:, : leaves[k].size].reshape(-1, *leaves[k].shape)
        at += len(line)
    numbers = iter(range(len(leaves)))
    return jax.tree.map(lambda _: found[next(numbers)], x)


def carried_in(x, axes, combine, identity):
    before = start = filled_with(x, identity)
    total = x
    for axis in reversed(axes):
        peers, index = (lax.axis_size(axis), lax.axis_index(axis))
        pieces = collected_together(
            jax.tree.map(
                lambda part, kind: part.astype(kind),
                total,
                (jnp.bfloat16, jnp.bfloat16, jnp.bfloat16, jnp.bfloat16),
            ),
            axis,
        )
        inside, total = (start, start)
        for k in range(peers):
            passed = k < index
            total = combine(
                total, jax.tree.map(lambda part, own: part[k].astype(own.dtype), pieces, x)
            )
            inside = jax.tree.map(lambda new, old: jnp.where(passed, new, old), total, inside)
        before = combine(inside, before)
    return before


def cut_along(x, dim, peers):
    shape = x.shape
    pieces = x.reshape(*shape[:dim], peers, shape[dim] // peers, *shape[dim + 1 :])
    return jnp.moveaxis(pieces, dim, 0)


def sum_at_owner(x, axis, dim):
    pieces = cut_along(x, dim, lax.axis_size(axis))
    arrived = lax.all_to_all(pieces, axis, split_axis=0, concat_axis=0, tiled=True)
    return arrived.astype(jnp.float32).sum(axis=0)


def copy_for_each(x, axis):
    copies = jnp.broadcast_to(x, (lax.axis_size(axis), *x.shape))
    return lax.all_to_all(copies, axis, split_axis=0, concat_axis=0, tiled=True)


def joined_along(pieces, dim):
    shape = list(pieces.shape[1:])
    shape[dim] *= pieces.shape[0]
    return jnp.moveaxis(pieces, 0, dim).reshape(shape)


def gathered_copies(x, axis, dim):
    pieces = copy_for_each(x, axis)
    return joined_along(pieces, dim)


def passed_along(value, axis, steps):
    count = lax.axis_size(axis)
    first, last = (max(0, -steps), min(count, count - steps))
    return lax.ppermute(value, axis, [(source, source + steps) for source in range(first, last)])


def rotate(block, positions):
    width = block.shape[-1]
    half = width // 2
    frequency = THETA ** (-(jnp.arange(half, dtype=jnp.float32) * 2.0 / width))
    angles = positions.astype(jnp.float32)[:, None] * frequency[None, :]
    cosine = jnp.cos(angles)[:, None, :]
    sine = jnp.sin(angles)[:, None, :]
    values = block.astype(jnp.float32)
    first = values[..., :half]
    second = values[..., half:]
    return jnp.concatenate(
        [first * cosine - second * sine, second * cosine + first * sine], axis=-1
    )


def block_step(state, inputs):
    query, keys, values, log_rate = inputs
    running = jnp.cumsum(log_rate, axis=1)
    length = running.shape[1]
    index = jnp.arange(length)
    lower = (index[:, None] >= index[None, :])[None]
    spread = jnp.where(
        lower, jnp.exp(jnp.where(lower, running[:, :, None] - running[:, None, :], 0.0)), 0.0
    )
    scores = (
        jnp.einsum("ihd,jhd->hij", query, keys, preferred_element_type=jnp.float32) * spread
    ).astype(jnp.bfloat16)
    inner = jnp.einsum("hij,jhe->ihe", scores, values, preferred_element_type=jnp.float32)
    lifted = query.astype(jnp.float32) * jnp.exp(running).T[:, :, None]
    cross = jnp.einsum("ihd,hde->ihe", lifted, state, precision=lax.Precision.HIGHEST)
    tail = running[:, -1:]
    scaled = (keys.astype(jnp.float32) * jnp.exp(tail - running).T[:, :, None]).astype(jnp.bfloat16)
    update = jnp.einsum("jhd,jhe->hde", scaled, values, preferred_element_type=jnp.float32)
    state = state * jnp.exp(tail)[:, :, None] + update
    return (state, inner + cross)


def kept_nearby_memory(query, keys, values, log_rate, head_dim, value_dim, offset):
    rows = query.shape[0]
    heads = query.shape[1] // head_dim
    positions = offset + jnp.arange(rows, dtype=jnp.int32)
    rotated_query = rotate(query.reshape(rows, heads, head_dim), positions).astype(jnp.bfloat16)
    rotated_keys = (
        rotate(keys.reshape(rows, heads, head_dim), positions) * head_dim ** (-0.5)
    ).astype(jnp.bfloat16)
    layer_groups_list = rows // BLOCK

    def split(array):
        return array.reshape(layer_groups_list, BLOCK, heads, array.shape[-1])

    rates = jnp.transpose(log_rate.reshape(heads, layer_groups_list, BLOCK), (1, 0, 2))
    start = jnp.zeros((heads, head_dim, value_dim), jnp.float32)
    inputs = (
        split(rotated_query),
        split(rotated_keys),
        split(values.reshape(rows, heads, value_dim)),
        rates,
    )
    state, outs = lax.scan(block_step, start, inputs)
    return (rotated_query, outs.reshape(rows, heads, value_dim), state)


def carried(rotated_query, log_rate, state_in):
    lifted = rotated_query.astype(jnp.float32) * jnp.exp(jnp.cumsum(log_rate, axis=1)).T[:, :, None]
    return jnp.einsum("ihd,hde->ihe", lifted, state_in, precision=lax.Precision.HIGHEST)


def gate_heads(retained, gain, gate):
    mean = jnp.mean(retained, axis=-1, keepdims=True)
    centred = retained - mean
    variance = jnp.mean(centred * centred, axis=-1, keepdims=True)
    normed = (centred * lax.rsqrt(variance + EPS)).reshape(retained.shape[0], -1)
    return (normed * gain.astype(jnp.float32) * jax.nn.silu(gate.astype(jnp.float32))).astype(
        jnp.bfloat16
    )


def scale_rows(rows, gain):
    return (
        rows
        * lax.rsqrt(jnp.mean(rows * rows, axis=-1, keepdims=True) + EPS)
        * gain.astype(jnp.float32)
    )


def causal_taps(upward, before, taps):
    width = taps.shape[0]
    total = upward.shape[0]
    padded_rows = jnp.concatenate([before, upward], axis=0).astype(jnp.float32)
    smooth = jnp.zeros((total, upward.shape[1]), jnp.float32)
    for tap_index in range(width):
        smooth = (
            smooth
            + taps[tap_index].astype(jnp.float32)[None, :]
            * padded_rows[tap_index : tap_index + total]
        )
    return smooth


def chain(earlier, later):
    return (
        earlier[0] * later[2] + later[0],
        earlier[1] * later[3] + later[1],
        earlier[2] * later[2],
        earlier[3] * later[3],
    )


def body(
    stream,
    wide_head_query,
    broad_attention_lookup_vectors,
    values_wide,
    query_narrow,
    keys_narrow,
    values_narrow,
    gate_wide,
    gate_narrow,
    log_decay,
    gain_wide,
    gain_narrow,
    out_wide,
    out_narrow,
    gain_mix,
    gain_pre,
    gain_post,
    weight_gate,
    weight_lin,
    weight_down,
    taps_gate,
    taps_lin,
):
    rows = wide_head_query.shape[0]
    offset = lax.axis_index(SP) * rows
    whole_gate, whole_lin, whole_down = sent_together(
        (weight_gate, weight_lin, weight_down), SP, 0, 1
    )
    rates_wide = log_decay[0]
    rates_narrow = log_decay[1]
    rot_wide, local_wide, state_wide = kept_nearby_memory(
        wide_head_query, broad_attention_lookup_vectors, values_wide, rates_wide, KW, VW, offset
    )
    rot_narrow, local_narrow, state_narrow = kept_nearby_memory(
        query_narrow, keys_narrow, values_narrow, rates_narrow, KN, VN, offset
    )
    decay_wide = jnp.exp(jnp.sum(rates_wide, axis=1))[:, None, None]
    decay_narrow = jnp.exp(jnp.sum(rates_narrow, axis=1))[:, None, None]
    identity = (
        jnp.zeros_like(state_wide),
        jnp.zeros_like(state_narrow),
        jnp.ones_like(decay_wide),
        jnp.ones_like(decay_narrow),
    )
    incoming = carried_in((state_wide, state_narrow, decay_wide, decay_narrow), SP, chain, identity)
    gated_wide = gate_heads(
        local_wide + carried(rot_wide, rates_wide, incoming[0]), gain_wide, gate_wide
    )
    gated_narrow = gate_heads(
        local_narrow + carried(rot_narrow, rates_narrow, incoming[1]), gain_narrow, gate_narrow
    )
    part_wide = jnp.dot(gated_wide, out_wide, preferred_element_type=jnp.float32)
    part_narrow = jnp.dot(gated_narrow, out_narrow, preferred_element_type=jnp.float32)
    mixed = sum_at_owner((part_wide + part_narrow).astype(jnp.bfloat16), "tp", 0)
    resid = (stream.astype(jnp.float32) + scale_rows(mixed, gain_mix)).astype(jnp.bfloat16)
    normed_in = scale_rows(resid.astype(jnp.float32), gain_pre).astype(jnp.bfloat16)
    normed_all = gathered_copies(normed_in, "tp", 0)
    up_gate = jnp.dot(normed_all, whole_gate, preferred_element_type=jnp.float32).astype(
        jnp.bfloat16
    )
    up_lin = jnp.dot(normed_all, whole_lin, preferred_element_type=jnp.float32).astype(jnp.bfloat16)
    reach = taps_gate.shape[0] - 1
    before_gate, before_lin = passed_along((up_gate[rows - reach :], up_lin[rows - reach :]), SP, 1)
    smooth_gate = causal_taps(up_gate, before_gate, taps_gate)
    smooth_lin = causal_taps(up_lin, before_lin, taps_lin)
    hidden = (jax.nn.silu(smooth_gate) * smooth_lin).astype(jnp.bfloat16)
    terms = lax.dot_general(
        hidden, whole_down, (((1,), (1,)), ((), ())), preferred_element_type=jnp.float32
    )
    fed = sum_at_owner(terms.astype(jnp.bfloat16), "tp", 0)
    return (resid.astype(jnp.float32) + scale_rows(fed, gain_post)).astype(jnp.bfloat16)


def solution(mesh):
    split = Mesh(mesh.devices.reshape(16, 4, mesh.shape["tp"]), ("sp_0", "sp_1", "tp"))
    return jax.shard_map(
        body,
        mesh=split,
        in_specs=(
            P(SP_TP, None),
            P(SP, "tp"),
            P(SP, "tp"),
            P(SP, "tp"),
            P(SP, "tp"),
            P(SP, "tp"),
            P(SP, "tp"),
            P(SP, "tp"),
            P(SP, "tp"),
            P(None, "tp", SP),
            P("tp"),
            P("tp"),
            P("tp", None),
            P("tp", None),
            P(),
            P(),
            P(),
            P(SP, "tp"),
            P(SP, "tp"),
            P(SP, "tp"),
            P(None, "tp"),
            P(None, "tp"),
        ),
        out_specs=P(SP_TP, None),
        check_vma=False,
    )
```

profile of v0, /device:TPU:1, one launch (start us, length us, event | category | flops | bytes accessed | tf_op | source)
XLA Modules:
  0.0 307.0 jit_solution(4947015568421868415)
XLA Ops:
  6.7 1.4 slice_bitcast_fusion
  10.2 0.7 bitcast_convert_fusion.2
  11.1 0.9 fusion.23
  15.5 0.8 bitcast_convert_fusion
  16.8 1.1 fusion.18
  17.9 10.9 %all-gather.2 = bf16[4,162,256]{2,1,0:T(8,128)(2,1)S(1)} all-gather(bf16[1,162,256]{2,1,0:T(8,128)(2,1)S(1)} %maximum_bitcast_fusion), channel_id=2, replica_groups=mesh['sp_0'=16,'sp_1'=4,'tp'=8] {'sp_1'}, dimensions={0}, use_global_device_ids=true | all-gather | bytes 414720 | tf_op jit(solution)/shard_map/all_gather | solution.py:43
  28.8 0.6 fusion.289
  31.3 0.6 fusion.288
  36.5 0.6 maximum_bitcast_fusion.1
  37.2 0.7 pad_maximum_fusion
  40.8 64.3 %all-gather.9.cloned.1.call-done = bf16[16,162,256]{2,1,0:T(8,128)(2,1)} async-done(((bf16[1,162,256]{2,1,0:T(8,128)(2,1)}), bf16[16,162,256]{2,1,0:T(8,128)(2,1)}) %all-gather.9.cloned.1.call-update) | async-done | bytes 1327120 | tf_op jit(solution)/shard_map/all_gather | solution.py:43
  105.1 0.9 fusion.284
  106.0 0.7 fusion.286
  116.8 1.1 select_add_fusion
  117.9 0.7 fusion.287
  129.5 2.1 fusion.290
  132.2 1.2 fusion.6
  133.5 15.4 %all-to-all-start = ((bf16[8,16,2048]{2,1,0:T(8,128)(2,1)}), bf16[8,16,2048]{2,1,0:T(8,128)(2,1)S(1)}, u32[]{:S(2)}, u32[]{:S(2)}) async-start(bf16[8,16,2048]{2,1,0:T(8,128)(2,1)} %bitcast.109), calls=%async_computation | async-start | bytes 1048576 | tf_op jit(solution)/shard_map/all_to_all | solution.py:84
  148.9 9.3 %all-to-all-done = bf16[8,16,2048]{2,1,0:T(8,128)(2,1)S(1)} async-done(((bf16[8,16,2048]{2,1,0:T(8,128)(2,1)}), bf16[8,16,2048]{2,1,0:T(8,128)(2,1)S(1)}, u32[]{:S(2)}, u32[]{:S(2)}) %all-to-all-start) | async-done | bytes 524320 | tf_op jit(solution)/shard_map/all_to_all | solution.py:84
  158.8 0.9 broadcast_in_dim.35
  159.6 4.4 %all-to-all-start.1 = ((bf16[8,16,2048]{2,1,0:T(8,128)(2,1)}), bf16[8,16,2048]{2,1,0:T(8,128)(2,1)S(1)}, u32[]{:S(2)}, u32[]{:S(2)}) async-start(bf16[8,16,2048]{2,1,0:T(8,128)(2,1)} %broadcast_in_dim.35), calls=%async_computation.1 | async-start | bytes 1048576 | tf_op jit(solution)/shard_map/all_to_all | solution.py:90
  164.0 9.3 %all-to-all-done.1 = bf16[8,16,2048]{2,1,0:T(8,128)(2,1)S(1)} async-done(((bf16[8,16,2048]{2,1,0:T(8,128)(2,1)}), bf16[8,16,2048]{2,1,0:T(8,128)(2,1)S(1)}, u32[]{:S(2)}, u32[]{:S(2)}) %all-to-all-start.1) | async-done | bytes 524320 | tf_op jit(solution)/shard_map/all_to_all | solution.py:90
  173.4 88.8 %all-gather.7.cloned.1.call-done = bf16[2048,1920]{1,0:T(8,128)(2,1)} async-done(((bf16[32,1920]{1,0:T(8,128)(2,1)}), bf16[2048,1920]{1,0:T(8,128)(2,1)}) %all-gather.7.cloned.1.call-update) | async-done | bytes 7864336 | tf_op jit(solution)/shard_map/all_gather | solution.py:26
  262.1 2.3 fusion.10
  264.5 1.8 collective-permute-start
  266.3 2.3 fusion.13
  268.6 2.8 collective-permute-start.1
  271.5 0.7 collective-permute-done.1
  272.2 3.6 %fusion.7 = bf16[128,2048]{1,0:T(8,128)(2,1)} fusion(bf16[2048,1920]{1,0:T(8,128)(2,1)} %all-gather.7.cloned.1.call-done, f32[130,640]{1,0:T(8,128)S(1)} %maximum_convert_fusion.1, f32[130,640]{1,0:T(8,128)S(1)} %maximum_convert_fusion, f32[640]{0:T(1024)S(1)} %get-tuple-element.42, f32[640]{0:T(1024)S(1)} %get-tuple-element.43, ...), kind=kOutput, calls=%fused_computation.8 | convolution fusion | flops 337117184 | bytes 5136384 | tf_op jit(solution)/shard_map/dot_general | solution.py:285
  275.8 14.0 %all-to-all-start.2 = ((bf16[8,16,2048]{2,1,0:T(8,128)(2,1)}), bf16[8,16,2048]{2,1,0:T(8,128)(2,1)S(1)}, u32[]{:S(2)}, u32[]{:S(2)}) async-start(bf16[8,16,2048]{2,1,0:T(8,128)(2,1)} %bitcast.111), calls=%async_computation.2 | async-start | bytes 1048576 | tf_op jit(solution)/shard_map/all_to_all | solution.py:84
  289.8 9.3 %all-to-all-done.2 = bf16[8,16,2048]{2,1,0:T(8,128)(2,1)S(1)} async-done(((bf16[8,16,2048]{2,1,0:T(8,128)(2,1)}), bf16[8,16,2048]{2,1,0:T(8,128)(2,1)S(1)}, u32[]{:S(2)}, u32[]{:S(2)}) %all-to-all-start.2) | async-done | bytes 524320 | tf_op jit(solution)/shard_map/all_to_all | solution.py:84
  299.4 0.7 fusion.45
  (107 shorter events, 7.4 us)
Async XLA Ops:
  6.5 125.3 %copy-start = (bf16[256,2048]{1,0:T(8,128)(2,1)S(1)}, bf16[256,2048]{1,0:T(8,128)(2,1)}, u32[]{:S(2)}) copy-start(bf16[256,2048]{1,0:T(8,128)(2,1)} %param.34) | copy-start | bytes 3145732
  6.5 122.5 %copy-start.9 = (bf16[128,128]{1,0:T(8,128)(2,1)S(1)}, bf16[128,128]{1,0:T(8,128)(2,1)}, u32[]{:S(2)}) copy-start(bf16[128,128]{1,0:T(8,128)(2,1)} %param.28) | copy-start | bytes 98308
  6.5 33.9 %copy-start.2 = (bf16[128,256]{1,0:T(8,128)(2,1)S(1)}, bf16[128,256]{1,0:T(8,128)(2,1)}, u32[]{:S(2)}) copy-start(bf16[128,256]{1,0:T(8,128)(2,1)} %param.25) | copy-start | bytes 196612
  6.5 30.7 %copy-start.7 = (bf16[32,640]{1,0:T(8,128)(2,1)S(1)}, bf16[32,640]{1,0:T(8,128)(2,1)}, u32[]{:S(2)}) copy-start(bf16[32,640]{1,0:T(8,128)(2,1)} %param.39) | copy-start | bytes 122884
  6.5 30.7 %copy-start.6 = (bf16[32,640]{1,0:T(8,128)(2,1)S(1)}, bf16[32,640]{1,0:T(8,128)(2,1)}, u32[]{:S(2)}) copy-start(bf16[32,640]{1,0:T(8,128)(2,1)} %param.40) | copy-start | bytes 122884
  6.5 30.7 %copy-start.5 = (bf16[32,640]{1,0:T(8,128)(2,1)S(1)}, bf16[32,640]{1,0:T(8,128)(2,1)}, u32[]{:S(2)}) copy-start(bf16[32,640]{1,0:T(8,128)(2,1)} %param.41) | copy-start | bytes 122884
  6.6 33.2 %copy-start.15 = (bf16[256]{0:T(256)(128)(2,1)S(1)}, bf16[256]{0:T(256)(128)(2,1)}, u32[]{:S(2)}) copy-start(bf16[256]{0:T(256)(128)(2,1)} %param.32) | copy-start | bytes 1540
  6.6 33.2 %copy-start.8 = (bf16[128,128]{1,0:T(8,128)(2,1)S(1)}, bf16[128,128]{1,0:T(8,128)(2,1)}, u32[]{:S(2)}) copy-start(bf16[128,128]{1,0:T(8,128)(2,1)} %param.30) | copy-start | bytes 98308
  6.6 33.4 %copy-start.16 = (bf16[128]{0:T(256)(128)(2,1)S(1)}, bf16[128]{0:T(256)(128)(2,1)}, u32[]{:S(2)}) copy-start(bf16[128]{0:T(256)(128)(2,1)} %param.33) | copy-start | bytes 772
  6.6 98.5 %all-gather.9.cloned.1.call-start = ((), (), s32[]{:S(2)}) async-start(), calls=%async_computation.4 | async-start | bytes 1462272 | tf_op jit(solution)/shard_map/all_gather | solution.py:43
  37.2 225.0 %all-gather.7.cloned.1.call-start = ((), (), s32[]{:S(2)}) async-start(), calls=%async_computation.3 | async-start | bytes 7987200 | tf_op jit(solution)/shard_map/all_gather | solution.py:26
  39.9 91.9 %copy-start.4 = (bf16[128,256]{1,0:T(8,128)(2,1)S(1)}, bf16[128,256]{1,0:T(8,128)(2,1)}, u32[]{:S(2)}) copy-start(bf16[128,256]{1,0:T(8,128)(2,1)} %param.29) | copy-start | bytes 196612
  129.5 2.7 copy-start.1
  131.8 17.1 %copy-start.12 = (bf16[2048]{0:T(1024)(128)(2,1)S(1)}, bf16[2048]{0:T(1024)(128)(2,1)}, u32[]{:S(2)}) copy-start(bf16[2048]{0:T(1024)(128)(2,1)} %param.36) | copy-start | bytes 12292
  131.8 17.0 %copy-start.13 = (bf16[2048]{0:T(1024)(128)(2,1)S(1)}, bf16[2048]{0:T(1024)(128)(2,1)}, u32[]{:S(2)}) copy-start(bf16[2048]{0:T(1024)(128)(2,1)} %param.37) | copy-start | bytes 12292
  131.8 26.6 %copy-start.3 = (bf16[16,2048]{1,0:T(8,128)(2,1)S(1)}, bf16[16,2048]{1,0:T(8,128)(2,1)}, u32[]{:S(2)}) copy-start(bf16[16,2048]{1,0:T(8,128)(2,1)} %param.22) | copy-start | bytes 196612
  132.2 31.8 %copy-start.10 = (bf16[3,640]{1,0:T(4,128)(2,1)S(1)}, bf16[3,640]{1,0:T(4,128)(2,1)}, u32[]{:S(2)}) copy-start(bf16[3,640]{1,0:T(4,128)(2,1)} %param.43) | copy-start | bytes 11524
  132.2 31.8 %copy-start.11 = (bf16[3,640]{1,0:T(4,128)(2,1)S(1)}, bf16[3,640]{1,0:T(4,128)(2,1)}, u32[]{:S(2)}) copy-start(bf16[3,640]{1,0:T(4,128)(2,1)} %param.42) | copy-start | bytes 11524
  133.5 24.8 %all-to-all-start = ((bf16[8,16,2048]{2,1,0:T(8,128)(2,1)}), bf16[8,16,2048]{2,1,0:T(8,128)(2,1)S(1)}, u32[]{:S(2)}, u32[]{:S(2)}) async-start(bf16[8,16,2048]{2,1,0:T(8,128)(2,1)} %bitcast.109), calls=%async_computation | async-start | bytes 1048576 | tf_op jit(solution)/shard_map/all_to_all | solution.py:84
  159.6 13.7 %all-to-all-start.1 = ((bf16[8,16,2048]{2,1,0:T(8,128)(2,1)}), bf16[8,16,2048]{2,1,0:T(8,128)(2,1)S(1)}, u32[]{:S(2)}, u32[]{:S(2)}) async-start(bf16[8,16,2048]{2,1,0:T(8,128)(2,1)} %broadcast_in_dim.35), calls=%async_computation.1 | async-start | bytes 1048576 | tf_op jit(solution)/shard_map/all_to_all | solution.py:90
  264.5 7.0 %collective-permute-start = (bf16[2,640]{1,0:T(2,128)(2,1)S(1)}, bf16[2,640]{1,0:T(2,128)(2,1)S(1)}, u32[]{:S(2)}, u32[]{:S(2)}) collective-permute-start(bf16[2,640]{1,0:T(2,128)(2,1)S(1)} %slice.702), channel_id=1, source_target_pairs={{0,8},{8,16},{16,24},{24,32},{32,40},{40,48},{48,56},{56,64},{64,7... | collective-permute-start | bytes 7688 | tf_op jit(solution)/shard_map/ppermute | solution.py:107
  268.6 3.6 %collective-permute-start.1 = (bf16[2,640]{1,0:T(2,128)(2,1)S(1)}, bf16[2,640]{1,0:T(2,128)(2,1)S(1)}, u32[]{:S(2)}, u32[]{:S(2)}) collective-permute-start(bf16[2,640]{1,0:T(2,128)(2,1)S(1)} %slice.706), channel_id=1, source_target_pairs={{0,8},{8,16},{16,24},{24,32},{32,40},{40,48},{48,56},{56,64},{64,7... | collective-permute-start | bytes 7688 | tf_op jit(solution)/shard_map/ppermute | solution.py:107
  272.2 17.6 %copy-start.14 = (bf16[2048]{0:T(1024)(128)(2,1)S(1)}, bf16[2048]{0:T(1024)(128)(2,1)}, u32[]{:S(2)}) copy-start(bf16[2048]{0:T(1024)(128)(2,1)} %param.38) | copy-start | bytes 12292
  275.8 23.4 %all-to-all-start.2 = ((bf16[8,16,2048]{2,1,0:T(8,128)(2,1)}), bf16[8,16,2048]{2,1,0:T(8,128)(2,1)S(1)}, u32[]{:S(2)}, u32[]{:S(2)}) async-start(bf16[8,16,2048]{2,1,0:T(8,128)(2,1)} %bitcast.111), calls=%async_computation.2 | async-start | bytes 1048576 | tf_op jit(solution)/shard_map/all_to_all | solution.py:84
Sparse Core Ops, SparseCore 0:
  37.3 67.7 all-gather.8
  108.0 154.0 all-gather.6
where the time goes:
time: 311 us; the launch traced here: 307 us
  waiting for transfers between devices  182 us (59%)
  between operations  44.7 us (14%)
  starting transfers between devices  38.5 us (12%)
  matrix products  14.9 us (5%)
  blocking collectives  10.9 us (4%)
  other arithmetic  10.1 us (3%)
  local copies, waits for them, and re-layouts  6.21 us (2%)
    all_gather x1, waiting for transfers between devices, sent_together(): lax.all_gather(both, axis, axis=dim, tiled=True)  88.8 us
    all_gather x1, waiting for transfers between devices, collected_together(): both, at, found = (lax.all_gather(jnp.concatenate(lines), axis), 0, {})  64.3 us
    all_to_all x2, starting transfers between devices, sum_at_owner(): lax.all_to_all(pieces, axis, split_axis=0, concat_axis=0, tiled=True)  29.4 us
    all_to_all x2, waiting for transfers between devices, sum_at_owner(): lax.all_to_all(pieces, axis, split_axis=0, concat_axis=0, tiled=True)  18.7 us
    all_gather x1, blocking collectives, collected_together(): both, at, found = (lax.all_gather(jnp.concatenate(lines), axis), 0, {})  10.9 us
    all_to_all x1, waiting for transfers between devices, copy_for_each(): return lax.all_to_all(copies, axis, split_axis=0, concat_axis=0, tiled=True)  9.32 us
  transfers between devices with their start and end apart: 7, of which 6 were waited for; matrix products, arithmetic and copies ran while one was open for 4% of the time, Pallas kernels for 0%

commit v1 on v0

v1 whole, which is shorter than its diff:
```python
import jax
import jax.numpy as jnp
import numpy as np
from jax import lax
from jax.experimental import pallas as pl
from jax.experimental.pallas import tpu as pltpu
from jax.sharding import Mesh
from jax.sharding import PartitionSpec as P

KW, VW, KN, VN = 128, 256, 64, 128
D = 2048
HALF = D // 2
UNITS = 160
BLOCK = 128
NZ, NY, NX = 16, 4, 4
EPS = 1e-06
THETA = 10000.0
MESH = pl.DeviceIdType.MESH
F32 = jnp.float32
BF16 = jnp.bfloat16
A = pl.ds(0, HALF)
B = pl.ds(HALF, HALF)


def mod(a, n):
    return lax.rem(a + n, n)


def dot(a, b, dims=((1,), (0,))):
    return lax.dot_general(a, b, (dims, ((), ())), preferred_element_type=F32)


def rms(v):
    return v * lax.rsqrt(jnp.mean(v * v, axis=-1, keepdims=True) + EPS)


def kernel(
    stream, qw, kw, vw, qn, kn, vn, gatew, gaten, decay, gainw, gainn, outw, outn,
    gain_mix, gain_pre, gain_post, wg, wl, wd, tg, tl, trig,
    out,
    wsend, weights, ssend, recv1, ssum, recv2, back, recv3, local, mix, mixr, msum, mixx,
    norm, taps, ups, halo_s, halo_r, down, downr, rsum, p1a, p1b, s2a, s2b, p2a, p2b, residual,
    ws_s, ws_r, up_s, up_r, dn_s, dn_r, st_s, st_r, hi_s, hi_r, bk_s, bk_r,
    mc_s, mc_r, mx_s, mx_r, agx_s, agx_r, agy_s, agy_r, ag2x_s, ag2x_r, ag2y_s, ag2y_r,
    da_s, da_r, db_s, db_r, ha_s, ha_r, dc_s, dc_r, r1a_s, r1a_r, r1b_s, r1b_r,
    r2a_s, r2a_r, r2b_s, r2b_r,
):
    z, y, x, c = (lax.axis_index(n) for n in ("z", "y", "x", "c"))
    zh, zl = z // 4, lax.rem(z, 4)
    me = zl * 4 + y
    sent = []

    def push(src, dst, ss, rs, **where):
        copy = pltpu.make_async_remote_copy(
            src_ref=src, dst_ref=dst, send_sem=ss, recv_sem=rs, device_id=where,
            device_id_type=MESH,
        )
        copy.start()
        sent.append(copy)

    def arrive(dst, ss, rs):
        pltpu.make_async_remote_copy(
            src_ref=dst, dst_ref=dst, send_sem=ss, recv_sem=rs, device_id={"c": 1 - c},
            device_id_type=MESH,
        ).wait_recv()

    barrier = pltpu.get_barrier_semaphore()

    def greet(**where):
        pl.semaphore_signal(barrier, inc=1, device_id=where, device_id_type=MESH)

    around = [(dz, dy) for dz in range(4) for dy in range(4) if dz or dy]

    def at_group(dz, dy, sign):
        return mod(zl + sign * dz, 4), mod(y + sign * dy, 4)

    for dz, dy in around:
        l, yy = at_group(dz, dy, 1)
        greet(z=zh * 4 + l, y=yy)
    for d in range(1, 4):
        greet(z=mod(zh + d, 4) * 4 + zl)
        greet(x=mod(x + d, NX))
    greet(c=1 - c)
    greet(z=mod(z + 1, NZ))
    greet(z=mod(z - 1, NZ))

    for j in range(NY):
        cols = slice(UNITS * j, UNITS * (j + 1))
        wsend[j] = jnp.concatenate(
            [
                wg[:, cols].astype(F32),
                wl[:, cols].astype(F32),
                wd[:, cols].astype(F32),
                jnp.zeros((32, 32), F32),
            ],
            axis=1,
        ).astype(BF16)
        taps[j, 0:3] = jnp.concatenate(
            [tg[:, cols].astype(F32), tl[:, cols].astype(F32), jnp.zeros((3, 64), F32)], axis=1
        )

    row = lax.broadcasted_iota(jnp.int32, (BLOCK, BLOCK), 0)
    col = lax.broadcasted_iota(jnp.int32, (BLOCK, BLOCK), 1)
    lower = row >= col
    position = (lax.broadcasted_iota(jnp.int32, (BLOCK, BLOCK), 0) + (z * 4 + y) * BLOCK).astype(F32)

    def turned(values, cosine, sine, width):
        half = width // 2
        swapped = jnp.concatenate([values[:, half:], values[:, :half]], axis=1)
        return values * cosine + swapped * sine

    def head(q, k, v, rate, which, width):
        angle = position[:, :width] * trig[2 * which : 2 * which + 1, :width]
        cosine = jnp.cos(angle)
        sine = jnp.sin(angle) * trig[2 * which + 1 : 2 * which + 2, :width]
        rot_q = turned(q[...].astype(F32), cosine, sine, width).astype(BF16)
        rot_k = (turned(k[...].astype(F32), cosine, sine, width) * width ** (-0.5)).astype(BF16)
        running = jnp.sum(jnp.where(lower, rate, 0.0), axis=1, keepdims=True)
        wide = jnp.broadcast_to(running, (BLOCK, BLOCK))
        across = wide.T
        spread = jnp.where(lower, jnp.exp(jnp.where(lower, wide - across, 0.0)), 0.0)
        last = running[BLOCK - 1 : BLOCK]
        scaled = rot_k.astype(F32) * jnp.exp(last - running)
        values = v[...]
        state = dot(scaled.T.astype(BF16), values)
        scores = (dot(rot_q, rot_k, ((1,), (1,))) * spread).astype(BF16)
        inner = dot(scores, values)
        lifted = (rot_q.astype(F32) * jnp.exp(running)).astype(BF16)
        return state, jnp.exp(last), inner, lifted

    state_w, decay_w, inner_w, lifted_w = head(qw, kw, vw, decay[0], 0, KW)
    state_n, decay_n, inner_n, lifted_n = head(qn, kn, vn, decay[1], 1, KN)
    sub = lax.broadcasted_iota(jnp.int32, (8, 128), 0)

    def hi_lo(w, n):
        w_hi = w.astype(BF16).astype(F32)
        n_hi = n.astype(BF16).astype(F32)
        parts = (w_hi, w - w_hi, n_hi, n - n_hi)
        tile = jnp.zeros((8, 128), F32)
        for i, part in enumerate(parts):
            tile = jnp.where(sub == i, part, tile)
        return tile

    tile = hi_lo(decay_w, decay_n)
    for i in range(16):
        narrow = state_n[8 * (i // 2) : 8 * (i // 2) + 8]
        ssend[i] = jnp.concatenate(
            [state_w[8 * i : 8 * i + 8], jnp.concatenate([narrow, tile], axis=1)], axis=0
        ).astype(BF16)
    local[:, 0:VW] = inner_w
    local[:, VW : VW + VN] = inner_n

    pl.semaphore_wait(barrier, 24)

    for d in range(1, 4):
        to = mod(y + d, NY)
        push(
            wsend.at[to], weights.at[z, pl.ds(pl.multiple_of(y * 32, 32), 32)],
            ws_s.at[d], ws_r.at[d], y=to,
        )
    for k, (dz, dy) in enumerate(around):
        l, yy = at_group(dz, dy, 1)
        push(ssend.at[l * 4 + yy], recv1.at[me], st_s.at[k], st_r.at[k], z=zh * 4 + l, y=yy)
    weights[z, pl.ds(pl.multiple_of(y * 32, 32), 32)] = wsend[y]
    recv1[me] = ssend[me]

    def ring(step):
        if step == 0:
            for d in range(1, 4):
                frm = mod(y - d, NY)
                arrive(weights.at[z, pl.ds(pl.multiple_of(frm * 32, 32), 32)], ws_s.at[d], ws_r.at[d])
        else:
            arrive(weights.at[mod(z - step, NZ)], up_s.at[step - 1], up_r.at[step - 1])
        if step < 8:
            blk = weights.at[mod(z - step, NZ)]
            push(blk, blk, up_s.at[step], up_r.at[step], z=mod(z + 1, NZ))
        if 0 < step < 8:
            arrive(weights.at[mod(z + step, NZ)], dn_s.at[step - 1], dn_r.at[step - 1])
        if step < 7:
            blk = weights.at[mod(z + step, NZ)]
            push(blk, blk, dn_s.at[step], dn_r.at[step], z=mod(z - 1, NZ))

    ring(0)

    for k, (dz, dy) in enumerate(around):
        l, yy = at_group(dz, dy, -1)
        arrive(recv1.at[l * 4 + yy], st_s.at[k], st_r.at[k])

    def factors(t):
        return t[8:9, 128:256] + t[9:10, 128:256], t[10:11, 128:256] + t[11:12, 128:256]

    pw, pn = jnp.zeros((8, 256), F32), jnp.zeros((8, 128), F32)
    fw, fn = jnp.ones((1, 128), F32), jnp.ones((1, 128), F32)
    before, scale = [], []
    for s in range(16):
        t = recv1[s].astype(F32)
        dw, dn = factors(t)
        before.append((pw, pn))
        scale.append((fw, fn))
        pw = pw * jnp.concatenate([dw, dw], axis=1) + t[0:8]
        pn = pn * dn + t[8:16, 0:128]
        fw, fn = fw * dw, fn * dn
    ssum[...] = jnp.concatenate(
        [pw, jnp.concatenate([pn, hi_lo(fw, fn)], axis=1)], axis=0
    ).astype(BF16)
    for d in range(1, 4):
        push(ssum, recv2.at[zh], hi_s.at[d], hi_r.at[d], z=mod(zh + d, 4) * 4 + zl)
    recv2[zh] = ssum[...]
    ring(1)
    for d in range(1, 4):
        arrive(recv2.at[mod(zh - d, 4)], hi_s.at[d], hi_r.at[d])
    iw, im = jnp.zeros((8, 256), F32), jnp.zeros((8, 128), F32)
    for h in range(3):
        t = recv2[h].astype(F32)
        dw, dn = factors(t)
        passed = h < zh
        iw = jnp.where(passed, iw * jnp.concatenate([dw, dw], axis=1) + t[0:8], iw)
        im = jnp.where(passed, im * dn + t[8:16, 0:128], im)
    for s in range(16):
        (bw, bn), (sw, sn) = before[s], scale[s]
        wide = iw * jnp.concatenate([sw, sw], axis=1) + bw
        narrow = im * sn + bn
        back[s] = jnp.concatenate(
            [wide, jnp.concatenate([narrow, jnp.zeros((8, 128), F32)], axis=1)], axis=0
        ).astype(BF16)
    for k, (dz, dy) in enumerate(around):
        l, yy = at_group(dz, dy, 1)
        push(back.at[l * 4 + yy], recv3.at[me], bk_s.at[k], bk_r.at[k], z=zh * 4 + l, y=yy)
    recv3[me] = back[me]
    ring(2)
    for k, (dz, dy) in enumerate(around):
        l, yy = at_group(dz, dy, -1)
        arrive(recv3.at[l * 4 + yy], bk_s.at[k], bk_r.at[k])
    into = [recv3[i].astype(F32) for i in range(16)]
    in_w = jnp.concatenate([t[0:8] for t in into], axis=0).astype(BF16)
    in_n = jnp.concatenate([t[8:16, 0:128] for t in into[::2]], axis=0).astype(BF16)

    def gated(retained, gain, gate):
        mean = jnp.mean(retained, axis=-1, keepdims=True)
        centred = retained - mean
        variance = jnp.mean(centred * centred, axis=-1, keepdims=True)
        g = gate[...].astype(F32)
        return (
            centred * lax.rsqrt(variance + EPS) * gain[...].astype(F32) * (g / (1.0 + jnp.exp(-g)))
        ).astype(BF16)

    gw = gated(local[:, 0:VW] + dot(lifted_w, in_w), gainw, gatew)
    gn = gated(local[:, VW : VW + VN] + dot(lifted_n, in_n), gainn, gaten)
    both = jnp.concatenate([gw, gn], axis=1)
    for n in range(4):
        cols = slice(512 * n, 512 * n + 512)
        weight = jnp.concatenate([outw[:, cols], outn[:, cols]], axis=0)
        part = dot(both, weight).astype(BF16)
        for g in range(8):
            mix[g % 2, g // 2, :, cols] = part[16 * g : 16 * g + 16]
    push(mix.at[1 - c], mixr, mc_s, mc_r, c=1 - c)
    ring(3)
    arrive(mixr, mc_s, mc_r)
    for i in range(NX):
        msum[i] = (mix[c, i].astype(F32) + mixr[i].astype(F32)).astype(BF16)
    for d in range(1, 4):
        to = mod(x + d, NX)
        push(msum.at[to], mixx.at[d - 1], mx_s.at[d], mx_r.at[d], x=to)
    ring(4)
    mixed = msum[x].astype(F32)
    for d in range(1, 4):
        arrive(mixx.at[d - 1], mx_s.at[d], mx_r.at[d])
        mixed = mixed + mixx[d - 1].astype(F32)
    resid = (stream[...].astype(F32) + rms(mixed) * gain_mix[...].astype(F32)).astype(BF16)
    residual[...] = resid
    norm[c, y, x] = (rms(resid.astype(F32)) * gain_pre[...].astype(F32)).astype(BF16)

    mine = norm.at[c, y, x]
    for d in range(1, 4):
        push(mine.at[:, A], mine.at[:, A], agx_s.at[d], agx_r.at[d], x=mod(x + d, NX))
        push(mine.at[:, B], mine.at[:, B], agy_s.at[d], agy_r.at[d], y=mod(y + d, NY))
    ring(5)
    for d in range(1, 4):
        arrive(norm.at[c, y, mod(x - d, NX), :, A], agx_s.at[d], agx_r.at[d])
    piece = norm.at[c, y, :, :, A]
    for d in range(1, 4):
        push(piece, piece, ag2y_s.at[d], ag2y_r.at[d], y=mod(y + d, NY))
    push(piece, piece, da_s.at[0], da_r.at[0], c=1 - c)
    for d in range(1, 4):
        arrive(norm.at[c, mod(y - d, NY), x, :, B], agy_s.at[d], agy_r.at[d])
    piece = norm.at[c, :, x, :, B]
    for d in range(1, 4):
        push(piece, piece, ag2x_s.at[d], ag2x_r.at[d], x=mod(x + d, NX))
    push(piece, piece, db_s.at[0], db_r.at[0], c=1 - c)
    ring(6)
    for d in range(1, 4):
        piece = norm.at[c, mod(y - d, NY), :, :, A]
        arrive(piece, ag2y_s.at[d], ag2y_r.at[d])
        push(piece, piece, da_s.at[d], da_r.at[d], c=1 - c)
        piece = norm.at[c, :, mod(x - d, NX), :, B]
        arrive(piece, ag2x_s.at[d], ag2x_r.at[d])
        push(piece, piece, db_s.at[d], db_r.at[d], c=1 - c)
    ring(7)
    for d in range(4):
        arrive(norm.at[1 - c, mod(y - d, NY), :, :, A], da_s.at[d], da_r.at[d])
        arrive(norm.at[1 - c, :, mod(x - d, NX), :, B], db_s.at[d], db_r.at[d])
    ring(8)

    def up(half):
        rows = norm[:, 2 * half : 2 * half + 2].reshape(256, D)
        full = weights[:, :, 0:384].reshape(D, 384)
        result = dot(rows, full).astype(BF16).astype(F32)
        for cc in range(2):
            for g in range(8):
                at = 8 + 256 * half + 32 * g + 16 * cc
                ups[at : at + 16] = result[128 * cc + 16 * g : 128 * cc + 16 * g + 16]

    up(1)
    halo_s[...] = ups[512:520].astype(BF16)
    push(halo_s, halo_r, ha_s, ha_r, z=mod(z + 1, NZ))
    up(0)

    def fed_down(half):
        tap = taps[y]
        hidden = []
        for r in range(2):
            base = 256 * half + 128 * r
            smooth = jnp.zeros((128, 384), F32)
            for j in range(3):
                smooth = smooth + tap[j : j + 1] * ups[6 + j + base : 6 + j + base + 128]
            gate = smooth[:, 0:160]
            hid = gate / (1.0 + jnp.exp(-gate)) * smooth[:, 160:320]
            hidden.append(
                jnp.concatenate(
                    [jnp.zeros((128, 64), F32), hid, jnp.zeros((128, 32), F32)], axis=1
                ).astype(BF16)
            )
        hid = jnp.concatenate(hidden, axis=0)
        for n in range(8):
            w = weights[2 * n : 2 * n + 2, :, 256:512].reshape(256, 256)
            part = dot(hid, w, ((1,), (1,))).astype(BF16)
            for g in range(16):
                down[g % 2, 2 * half + g // 8, (g // 2) % 4, :, 256 * n : 256 * n + 256] = part[
                    16 * g : 16 * g + 16
                ]
        push(
            down.at[1 - c, pl.ds(2 * half, 2)], downr.at[pl.ds(2 * half, 2)],
            dc_s.at[half], dc_r.at[half], c=1 - c,
        )

    def pair_sum(half):
        arrive(downr.at[pl.ds(2 * half, 2)], dc_s.at[half], dc_r.at[half])
        for j in range(2 * half, 2 * half + 2):
            for i in range(NX):
                rsum[j, i] = (down[c, j, i].astype(F32) + downr[j, i].astype(F32)).astype(BF16)

    fed_down(1)
    arrive(halo_r, ha_s, ha_r)
    ups[0:8] = jnp.where(z > 0, halo_r[...].astype(F32), 0.0)
    fed_down(0)
    pair_sum(1)
    pair_sum(0)
    for d in range(1, 4):
        to = mod(x + d, NX)
        push(rsum.at[:, to, :, A], p1a.at[d - 1], r1a_s.at[d], r1a_r.at[d], x=to)
        to = mod(y + d, NY)
        push(rsum.at[to, :, :, B], p1b.at[d - 1], r1b_s.at[d], r1b_r.at[d], y=to)
    for d in range(1, 4):
        arrive(p1a.at[d - 1], r1a_s.at[d], r1a_r.at[d])
    for i in range(4):
        total = rsum[i, x, :, 0:HALF].astype(F32)
        for d in range(3):
            total = total + p1a[d, i].astype(F32)
        s2a[i] = total.astype(BF16)
    for d in range(1, 4):
        to = mod(y + d, NY)
        push(s2a.at[to], p2a.at[d - 1], r2a_s.at[d], r2a_r.at[d], y=to)
    for d in range(1, 4):
        arrive(p1b.at[d - 1], r1b_s.at[d], r1b_r.at[d])
    for i in range(4):
        total = rsum[y, i, :, HALF:D].astype(F32)
        for d in range(3):
            total = total + p1b[d, i].astype(F32)
        s2b[i] = total.astype(BF16)
    for d in range(1, 4):
        to = mod(x + d, NX)
        push(s2b.at[to], p2b.at[d - 1], r2b_s.at[d], r2b_r.at[d], x=to)
    fa = s2a[y].astype(F32)
    for d in range(1, 4):
        arrive(p2a.at[d - 1], r2a_s.at[d], r2a_r.at[d])
        fa = fa + p2a[d - 1].astype(F32)
    fb = s2b[x].astype(F32)
    for d in range(1, 4):
        arrive(p2b.at[d - 1], r2b_s.at[d], r2b_r.at[d])
        fb = fb + p2b[d - 1].astype(F32)
    fed = jnp.concatenate([fa, fb], axis=1)
    out[...] = (residual[...].astype(F32) + rms(fed) * gain_post[...].astype(F32)).astype(BF16)
    for copy in sent:
        copy.wait_send()


def body(*args):
    args = list(args)
    for i in (10, 11, 14, 15, 16):
        args[i] = args[i].reshape(1, -1)
    freq_w = THETA ** (-(np.arange(64, dtype=np.float32) * 2.0 / 128))
    freq_n = THETA ** (-(np.arange(32, dtype=np.float32) * 2.0 / 64))
    trig = np.zeros((8, 128), np.float32)
    trig[0] = np.tile(freq_w, 2)
    trig[1] = np.where(np.arange(128) < 64, -1.0, 1.0)
    trig[2] = np.tile(freq_n, 4)
    trig[3] = np.where(np.arange(128) < 32, -1.0, 1.0)
    args.append(jnp.asarray(trig))
    vm = pltpu.VMEM
    sem = pltpu.SemaphoreType.DMA
    scratch = [
        vm((4, 32, 512), BF16),
        vm((NZ, 128, 512), BF16),
        vm((16, 16, 256), BF16),
        vm((16, 16, 256), BF16),
        vm((16, 256), BF16),
        vm((4, 16, 256), BF16),
        vm((16, 16, 256), BF16),
        vm((16, 16, 256), BF16),
        vm((BLOCK, VW + VN), F32),
        vm((2, 4, 16, D), BF16),
        vm((4, 16, D), BF16),
        vm((4, 16, D), BF16),
        vm((3, 16, D), BF16),
        vm((2, 4, 4, 16, D), BF16),
        vm((4, 8, 384), F32),
        vm((520, 384), F32),
        vm((8, 384), BF16),
        vm((8, 384), BF16),
        vm((2, 4, 4, 16, D), BF16),
        vm((4, 4, 16, D), BF16),
        vm((4, 4, 16, D), BF16),
        vm((3, 4, 16, HALF), BF16),
        vm((3, 4, 16, HALF), BF16),
        vm((4, 16, HALF), BF16),
        vm((4, 16, HALF), BF16),
        vm((3, 16, HALF), BF16),
        vm((3, 16, HALF), BF16),
        vm((16, D), BF16),
        sem((4,)), sem((4,)),
        sem((8,)), sem((8,)),
        sem((7,)), sem((7,)),
        sem((15,)), sem((15,)),
        sem((4,)), sem((4,)),
        sem((15,)), sem((15,)),
        sem, sem,
        sem((4,)), sem((4,)),
        sem((4,)), sem((4,)),
        sem((4,)), sem((4,)),
        sem((4,)), sem((4,)),
        sem((4,)), sem((4,)),
        sem((4,)), sem((4,)),
        sem((4,)), sem((4,)),
        sem, sem,
        sem((2,)), sem((2,)),
        sem((4,)), sem((4,)),
        sem((4,)), sem((4,)),
        sem((4,)), sem((4,)),
        sem((4,)), sem((4,)),
    ]
    return pl.pallas_call(
        kernel,
        out_shape=jax.ShapeDtypeStruct((16, D), BF16),
        in_specs=[pl.BlockSpec(memory_space=vm)] * len(args),
        out_specs=pl.BlockSpec(memory_space=vm),
        scratch_shapes=scratch,
        compiler_params=pltpu.CompilerParams(
            collective_id=0, has_side_effects=True, vmem_limit_bytes=60 * 1024 * 1024
        ),
        name="layer",
    )(*args)


def solution(mesh):
    split = Mesh(mesh.devices.reshape(NZ, NY, NX, 2), ("z", "y", "x", "c"))
    sp, tp = ("z", "y"), ("x", "c")
    both = ("z", "y", "x", "c")
    rows, heads = P(sp, tp), P(tp)
    return jax.shard_map(
        body,
        mesh=split,
        in_specs=(
            P(both, None), rows, rows, rows, rows, rows, rows, rows, rows,
            P(None, tp, sp), heads, heads, P(tp, None), P(tp, None), P(), P(), P(),
            rows, rows, rows, P(None, tp), P(None, tp),
        ),
        out_specs=P(both, None),
        check_vma=False,
    )
```

time: 311 us -> 90.5 us (0.29); the launches traced: 307 us -> 90.2 us
  waiting for transfers between devices: 182 us -> 0 us
  Pallas kernels: 0 us -> 83.5 us
  between operations: 44.7 us -> 0.02 us
  starting transfers between devices: 38.5 us -> 0 us
  matrix products: 14.9 us -> 0 us
  blocking collectives: 10.9 us -> 0 us
  other arithmetic: 10.1 us -> 0 us
    all_gather x2 -> x0, waiting for transfers between devices: 153 us -> none  [the longest x1 88.8 us: sent_together(): lax.all_gather(both, axis, axis=dim, tiled=True)]
    pallas_call x0 -> x1, Pallas kernels: none -> 83.5 us  [body(): pl.pallas_call(kernel, out_shape=jax.ShapeDtypeStruct((16, D), BF16), in_...]
    all_to_all x3 -> x0, starting transfers between devices: 33.8 us -> none  [the longest x2 29.4 us: sum_at_owner(): lax.all_to_all(pieces, axis, split_axis=0, concat_axis=0, tiled=True)]
    all_to_all x3 -> x0, waiting for transfers between devices: 28 us -> none  [the longest x2 18.7 us: sum_at_owner(): lax.all_to_all(pieces, axis, split_axis=0, concat_axis=0, tiled=True)]
    dot_general x11 -> x0, matrix products: 14.9 us -> none  [the longest x1 3.59 us: body(): lax.dot_general(hidden, whole_down, (((1,), (1,)), ((), ())), preferred_e...]
    all_gather x1 -> x0, blocking collectives: 10.9 us -> none  [collected_together(): both, at, found = (lax.all_gather(jnp.concatenate(lines), axis), 0, {})]
    slice x10 -> x0, local copies, waits for them, and re-layouts: 4.62 us -> none  [the longest x4 2.5 us: carried_in(): part[k].astype(own.dtype)]
    ppermute x2 -> x0, starting transfers between devices: 4.6 us -> none  [passed_along(): lax.ppermute(value, axis, [(source, source + steps) for source in range(f...]
  transfers between devices with their start and end apart: 7 -> 0, of which waited for: 6 -> 0; matrix products, arithmetic and copies ran while one was open for 4% -> 0% of each run, Pallas kernels for 0% -> 0%
where the time goes in v1:
time: 90.5 us; the launch traced here: 90.2 us
  Pallas kernels  83.5 us (92%)
  local copies, waits for them, and re-layouts  6.7 us (7%)
    pallas_call x1, Pallas kernels, body(): pl.pallas_call(kernel, out_shape=jax.ShapeDtypeStruct((16, D), BF16), in_...  83.5 us
    unnamed x13, local copies, waits for them, and re-layouts  3.67 us
    reshape x4, local copies, waits for them, and re-layouts, body(): args[i] = args[i].reshape(1, -1)  3.04 us

profile of v1, /device:TPU:1, one launch (start us, length us, event | category | flops | bytes accessed | tf_op | source)
XLA Modules:
  0.0 90.2 jit_solution(14560015913148185462)
XLA Ops:
  0.0 0.0 copy-start.4
  0.0 0.7 copy-done.4
  0.7 0.0 copy-start.2
  0.7 0.5 reshape.15.gainw
  1.2 0.0 copy-start
  1.2 1.3 %reshape.17.gain_mix = bf16[1,2048]{1,0:T(2,128)(2,1)} reshape(bf16[2048]{0:T(1024)(128)(2,1)} %param.37) | data formatting | bytes 8192 | tf_op jit(solution)/shard_map/reshape | solution.py:400
  2.5 0.0 copy-done.2
  2.5 0.0 copy-start.3
  2.5 0.6 reshape.18.gain_pre
  3.1 0.1 copy-done.3
  3.2 0.6 reshape.19.gain_post
  3.8 0.0 copy-done
  3.8 0.0 copy-start.1
  3.8 0.7 copy.24.qn
  4.5 0.0 copy-done.1
  4.5 0.7 copy.25.kn
  5.2 83.5 %layer.1 = bf16[16,2048]{1,0:T(8,128)(2,1)} custom-call(bf16[16,2048]{1,0:T(8,128)(2,1)} %stream.1, bf16[128,128]{1,0:T(8,128)(2,1)} %qw.1, bf16[128,128]{1,0:T(8,128)(2,1)} %kw.1, bf16[128,256]{1,0:T(8,128)(2,1)} %vw.1, bf16[128,64]{1,0:T(8,128)(2,1)} %copy.24.qn, bf16[128,64]{1,0:T(8,128)(2,1)} %copy.25.kn, bf16[128,128]{1,0:T(8,128)(2,1)} %vn.1, ...), custom_call_target="tpu_custom_call" | custom-call | tf_op jit(solution)/shard_map/layer/pallas_call | solution.py:461
  88.7 1.5 %copy.27 = bf16[16,2048]{1,0:T(8,128)(2,1)} copy(bf16[16,2048]{1,0:T(8,128)(2,1)} %layer.1) | data formatting | bytes 131072
Async XLA Ops:
  0.0 0.7 copy-start.4
  0.7 1.8 %copy-start.2 = (bf16[2048]{0:T(1024)(128)(2,1)S(1)}, bf16[2048]{0:T(1024)(128)(2,1)}, u32[]{:S(2)}) copy-start(bf16[2048]{0:T(1024)(128)(2,1)} %param.38) | copy-start | bytes 12292
  1.2 2.6 %copy-start = (bf16[128,64]{0,1:T(8,128)(2,1)S(1)}, bf16[128,64]{0,1:T(8,128)(2,1)}, u32[]{:S(2)}) copy-start(bf16[128,64]{0,1:T(8,128)(2,1)} %param.27) | copy-start | bytes 49156
  2.5 0.7 copy-start.3
  3.8 0.7 copy-start.1

commit v2 on v1

--- a/solution.py
+++ b/solution.py
@@ -28,6 +28,10 @@
 
 def dot(a, b, dims=((1,), (0,))):
     return lax.dot_general(a, b, (dims, ((), ())), preferred_element_type=F32)
+
+
+def line(gain):
+    return gain[...].astype(F32).reshape(1, -1)
 
 
 def rms(v):
@@ -113,8 +117,8 @@
         angle = position[:, :width] * trig[2 * which : 2 * which + 1, :width]
         cosine = jnp.cos(angle)
         sine = jnp.sin(angle) * trig[2 * which + 1 : 2 * which + 2, :width]
-        rot_q = turned(q[...].astype(F32), cosine, sine, width).astype(BF16)
-        rot_k = (turned(k[...].astype(F32), cosine, sine, width) * width ** (-0.5)).astype(BF16)
+        rot_q = turned(q, cosine, sine, width).astype(BF16)
+        rot_k = (turned(k, cosine, sine, width) * width ** (-0.5)).astype(BF16)
         running = jnp.sum(jnp.where(lower, rate, 0.0), axis=1, keepdims=True)
         wide = jnp.broadcast_to(running, (BLOCK, BLOCK))
         across = wide.T
@@ -128,8 +132,12 @@
         lifted = (rot_q.astype(F32) * jnp.exp(running)).astype(BF16)
         return state, jnp.exp(last), inner, lifted
 
-    state_w, decay_w, inner_w, lifted_w = head(qw, kw, vw, decay[0], 0, KW)
-    state_n, decay_n, inner_n, lifted_n = head(qn, kn, vn, decay[1], 1, KN)
+    state_w, decay_w, inner_w, lifted_w = head(
+        qw[...].astype(F32), kw[...].astype(F32), vw, decay[0], 0, KW
+    )
+    state_n, decay_n, inner_n, lifted_n = head(
+        qn[...].astype(F32).T, kn[...].astype(F32).T, vn, decay[1], 1, KN
+    )
     sub = lax.broadcasted_iota(jnp.int32, (8, 128), 0)
 
     def hi_lo(w, n):
@@ -241,7 +249,7 @@
         variance = jnp.mean(centred * centred, axis=-1, keepdims=True)
         g = gate[...].astype(F32)
         return (
-            centred * lax.rsqrt(variance + EPS) * gain[...].astype(F32) * (g / (1.0 + jnp.exp(-g)))
+            centred * lax.rsqrt(variance + EPS) * line(gain) * (g / (1.0 + jnp.exp(-g)))
         ).astype(BF16)
 
     gw = gated(local[:, 0:VW] + dot(lifted_w, in_w), gainw, gatew)
@@ -266,9 +274,9 @@
     for d in range(1, 4):
         arrive(mixx.at[d - 1], mx_s.at[d], mx_r.at[d])
         mixed = mixed + mixx[d - 1].astype(F32)
-    resid = (stream[...].astype(F32) + rms(mixed) * gain_mix[...].astype(F32)).astype(BF16)
+    resid = (stream[...].astype(F32) + rms(mixed) * line(gain_mix)).astype(BF16)
     residual[...] = resid
-    norm[c, y, x] = (rms(resid.astype(F32)) * gain_pre[...].astype(F32)).astype(BF16)
+    norm[c, y, x] = (rms(resid.astype(F32)) * line(gain_pre)).astype(BF16)
 
     mine = norm.at[c, y, x]
     for d in range(1, 4):
@@ -389,15 +397,14 @@
         arrive(p2b.at[d - 1], r2b_s.at[d], r2b_r.at[d])
         fb = fb + p2b[d - 1].astype(F32)
     fed = jnp.concatenate([fa, fb], axis=1)
-    out[...] = (residual[...].astype(F32) + rms(fed) * gain_post[...].astype(F32)).astype(BF16)
+    out[...] = (residual[...].astype(F32) + rms(fed) * line(gain_post)).astype(BF16)
     for copy in sent:
         copy.wait_send()
 
 
 def body(*args):
     args = list(args)
-    for i in (10, 11, 14, 15, 16):
-        args[i] = args[i].reshape(1, -1)
+    args[4], args[5] = args[4].T, args[5].T
     freq_w = THETA ** (-(np.arange(64, dtype=np.float32) * 2.0 / 128))
     freq_n = THETA ** (-(np.arange(32, dtype=np.float32) * 2.0 / 64))
     trig = np.zeros((8, 128), np.float32)

time: 90.5 us -> 85.2 us (0.941)
  local copies, waits for them, and re-layouts: 6.7 us -> 1.47 us
    reshape x4 -> x0, local copies, waits for them, and re-layouts: 3.04 us -> none  [body(): args[i] = args[i].reshape(1, -1)]
    unnamed x13 -> x1, local copies, waits for them, and re-layouts: 3.67 us -> 1.47 us
where the time goes in v2:
time: 85.2 us; the launch traced here: 85 us
  Pallas kernels  83.5 us (98%)
  local copies, waits for them, and re-layouts  1.47 us (2%)
    pallas_call x1, Pallas kernels, body(): pl.pallas_call(kernel, out_shape=jax.ShapeDtypeStruct((16, D), BF16), in_...  83.5 us

profile of v2, /device:TPU:1, one launch (start us, length us, event | category | flops | bytes accessed | tf_op | source)
XLA Modules:
  0.0 85.0 jit_solution(6080918960347483278)
XLA Ops:
  0.0 83.5 %layer.1 = bf16[16,2048]{1,0:T(8,128)(2,1)} custom-call(bf16[16,2048]{1,0:T(8,128)(2,1)} %stream.1, bf16[128,128]{1,0:T(8,128)(2,1)} %qw.1, bf16[128,128]{1,0:T(8,128)(2,1)} %kw.1, bf16[128,256]{1,0:T(8,128)(2,1)} %vw.1, bf16[64,128]{1,0:T(8,128)(2,1)} %bitcast.2, bf16[64,128]{1,0:T(8,128)(2,1)} %bitcast.3, bf16[128,128]{1,0:T(8,128)(2,1)} %vn.1, ...), custom_call_target="tpu_custom_call" | custom-call | tf_op jit(solution)/shard_map/layer/pallas_call | solution.py:468
  83.5 1.5 %copy.25 = bf16[16,2048]{1,0:T(8,128)(2,1)} copy(bf16[16,2048]{1,0:T(8,128)(2,1)} %layer.1) | data formatting | bytes 131072

commit v3 on v2

--- a/solution.py
+++ b/solution.py
@@ -41,13 +41,13 @@
 def kernel(
     stream, qw, kw, vw, qn, kn, vn, gatew, gaten, decay, gainw, gainn, outw, outn,
     gain_mix, gain_pre, gain_post, wg, wl, wd, tg, tl, trig,
-    out,
+    residual, out,
     wsend, weights, ssend, recv1, ssum, recv2, back, recv3, local, mix, mixr, msum, mixx,
-    norm, taps, ups, halo_s, halo_r, down, downr, rsum, p1a, p1b, s2a, s2b, p2a, p2b, residual,
+    norm, taps, ups, halo_s, halo_r, down, downr, rsum, p1a, p1b, s2a, s2b, p2a, p2b, acc,
     ws_s, ws_r, up_s, up_r, dn_s, dn_r, st_s, st_r, hi_s, hi_r, bk_s, bk_r,
     mc_s, mc_r, mx_s, mx_r, agx_s, agx_r, agy_s, agy_r, ag2x_s, ag2x_r, ag2y_s, ag2y_r,
     da_s, da_r, db_s, db_r, ha_s, ha_r, dc_s, dc_r, r1a_s, r1a_r, r1b_s, r1b_r,
-    r2a_s, r2a_r, r2b_s, r2b_r,
+    r2a_s, r2a_r, r2b_s, r2b_r, loads,
 ):
     z, y, x, c = (lax.axis_index(n) for n in ("z", "y", "x", "c"))
     zh, zl = z // 4, lax.rem(z, 4)
@@ -87,6 +87,15 @@
     greet(c=1 - c)
     greet(z=mod(z + 1, NZ))
     greet(z=mod(z - 1, NZ))
+
+    for load in loads.values():
+        load.start()
+
+    def need(*which):
+        for i in which:
+            loads[i].wait()
+
+    need(17, 18, 19, 20, 21)
 
     for j in range(NY):
         cols = slice(UNITS * j, UNITS * (j + 1))
@@ -103,6 +112,7 @@
             [tg[:, cols].astype(F32), tl[:, cols].astype(F32), jnp.zeros((3, 64), F32)], axis=1
         )
 
+    need(1, 2, 3, 4, 5, 6, 9, 22)
     row = lax.broadcasted_iota(jnp.int32, (BLOCK, BLOCK), 0)
     col = lax.broadcasted_iota(jnp.int32, (BLOCK, BLOCK), 1)
     lower = row >= col
@@ -172,24 +182,28 @@
     weights[z, pl.ds(pl.multiple_of(y * 32, 32), 32)] = wsend[y]
     recv1[me] = ssend[me]
 
-    def ring(step):
-        if step == 0:
-            for d in range(1, 4):
-                frm = mod(y - d, NY)
-                arrive(weights.at[z, pl.ds(pl.multiple_of(frm * 32, 32), 32)], ws_s.at[d], ws_r.at[d])
-        else:
-            arrive(weights.at[mod(z - step, NZ)], up_s.at[step - 1], up_r.at[step - 1])
+    def ring_start():
+        for d in range(1, 4):
+            frm = mod(y - d, NY)
+            arrive(weights.at[z, pl.ds(pl.multiple_of(frm * 32, 32), 32)], ws_s.at[d], ws_r.at[d])
+        for h in range(2):
+            blk = weights.at[z, pl.ds(64 * h, 64)]
+            push(blk, blk, up_s.at[h], up_r.at[h], z=mod(z + 1, NZ))
+            push(blk, blk, dn_s.at[h], dn_r.at[h], z=mod(z - 1, NZ))
+
+    def ring(step, h):
+        k = 2 * step + h
+        blk = weights.at[mod(z - step, NZ), pl.ds(64 * h, 64)]
+        arrive(blk, up_s.at[k - 2], up_r.at[k - 2])
         if step < 8:
-            blk = weights.at[mod(z - step, NZ)]
-            push(blk, blk, up_s.at[step], up_r.at[step], z=mod(z + 1, NZ))
-        if 0 < step < 8:
-            arrive(weights.at[mod(z + step, NZ)], dn_s.at[step - 1], dn_r.at[step - 1])
-        if step < 7:
-            blk = weights.at[mod(z + step, NZ)]
-            push(blk, blk, dn_s.at[step], dn_r.at[step], z=mod(z - 1, NZ))
-
-    ring(0)
-
+            push(blk, blk, up_s.at[k], up_r.at[k], z=mod(z + 1, NZ))
+            blk = weights.at[mod(z + step, NZ), pl.ds(64 * h, 64)]
+            arrive(blk, dn_s.at[k - 2], dn_r.at[k - 2])
+            if step < 7:
+                push(blk, blk, dn_s.at[k], dn_r.at[k], z=mod(z - 1, NZ))
+
+
+    ring_start()
     for k, (dz, dy) in enumerate(around):
         l, yy = at_group(dz, dy, -1)
         arrive(recv1.at[l * 4 + yy], st_s.at[k], st_r.at[k])
@@ -214,7 +228,9 @@
     for d in range(1, 4):
         push(ssum, recv2.at[zh], hi_s.at[d], hi_r.at[d], z=mod(zh + d, 4) * 4 + zl)
     recv2[zh] = ssum[...]
-    ring(1)
+    ring(1, 0)
+    ring(1, 1)
+    ring(2, 0)
     for d in range(1, 4):
         arrive(recv2.at[mod(zh - d, 4)], hi_s.at[d], hi_r.at[d])
     iw, im = jnp.zeros((8, 256), F32), jnp.zeros((8, 128), F32)
@@ -235,10 +251,13 @@
         l, yy = at_group(dz, dy, 1)
         push(back.at[l * 4 + yy], recv3.at[me], bk_s.at[k], bk_r.at[k], z=zh * 4 + l, y=yy)
     recv3[me] = back[me]
-    ring(2)
+    ring(2, 1)
+    ring(3, 0)
+    ring(3, 1)
     for k, (dz, dy) in enumerate(around):
         l, yy = at_group(dz, dy, -1)
         arrive(recv3.at[l * 4 + yy], bk_s.at[k], bk_r.at[k])
+    need(0, 7, 8, 10, 11, 12, 13, 14, 15, 16)
     into = [recv3[i].astype(F32) for i in range(16)]
     in_w = jnp.concatenate([t[0:8] for t in into], axis=0).astype(BF16)
     in_n = jnp.concatenate([t[8:16, 0:128] for t in into[::2]], axis=0).astype(BF16)
@@ -262,14 +281,18 @@
         for g in range(8):
             mix[g % 2, g // 2, :, cols] = part[16 * g : 16 * g + 16]
     push(mix.at[1 - c], mixr, mc_s, mc_r, c=1 - c)
-    ring(3)
+    ring(4, 0)
+    ring(4, 1)
     arrive(mixr, mc_s, mc_r)
     for i in range(NX):
         msum[i] = (mix[c, i].astype(F32) + mixr[i].astype(F32)).astype(BF16)
     for d in range(1, 4):
         to = mod(x + d, NX)
         push(msum.at[to], mixx.at[d - 1], mx_s.at[d], mx_r.at[d], x=to)
-    ring(4)
+    ring(5, 0)
+    ring(5, 1)
+    ring(6, 0)
+    ring(6, 1)
     mixed = msum[x].astype(F32)
     for d in range(1, 4):
         arrive(mixx.at[d - 1], mx_s.at[d], mx_r.at[d])
@@ -279,49 +302,98 @@
     norm[c, y, x] = (rms(resid.astype(F32)) * line(gain_pre)).astype(BF16)
 
     mine = norm.at[c, y, x]
-    for d in range(1, 4):
+    for d in (2, 1, 3):
         push(mine.at[:, A], mine.at[:, A], agx_s.at[d], agx_r.at[d], x=mod(x + d, NX))
         push(mine.at[:, B], mine.at[:, B], agy_s.at[d], agy_r.at[d], y=mod(y + d, NY))
-    ring(5)
-    for d in range(1, 4):
-        arrive(norm.at[c, y, mod(x - d, NX), :, A], agx_s.at[d], agx_r.at[d])
-    piece = norm.at[c, y, :, :, A]
-    for d in range(1, 4):
-        push(piece, piece, ag2y_s.at[d], ag2y_r.at[d], y=mod(y + d, NY))
-    push(piece, piece, da_s.at[0], da_r.at[0], c=1 - c)
-    for d in range(1, 4):
-        arrive(norm.at[c, mod(y - d, NY), x, :, B], agy_s.at[d], agy_r.at[d])
-    piece = norm.at[c, :, x, :, B]
-    for d in range(1, 4):
-        push(piece, piece, ag2x_s.at[d], ag2x_r.at[d], x=mod(x + d, NX))
-    push(piece, piece, db_s.at[0], db_r.at[0], c=1 - c)
-    ring(6)
-    for d in range(1, 4):
-        piece = norm.at[c, mod(y - d, NY), :, :, A]
-        arrive(piece, ag2y_s.at[d], ag2y_r.at[d])
-        push(piece, piece, da_s.at[d], da_r.at[d], c=1 - c)
-        piece = norm.at[c, :, mod(x - d, NX), :, B]
-        arrive(piece, ag2x_s.at[d], ag2x_r.at[d])
-        push(piece, piece, db_s.at[d], db_r.at[d], c=1 - c)
-    ring(7)
-    for d in range(4):
-        arrive(norm.at[1 - c, mod(y - d, NY), :, :, A], da_s.at[d], da_r.at[d])
-        arrive(norm.at[1 - c, :, mod(x - d, NX), :, B], db_s.at[d], db_r.at[d])
-    ring(8)
-
-    def up(half):
-        rows = norm[:, 2 * half : 2 * half + 2].reshape(256, D)
-        full = weights[:, :, 0:384].reshape(D, 384)
-        result = dot(rows, full).astype(BF16).astype(F32)
-        for cc in range(2):
-            for g in range(8):
-                at = 8 + 256 * half + 32 * g + 16 * cc
-                ups[at : at + 16] = result[128 * cc + 16 * g : 128 * cc + 16 * g + 16]
-
-    up(1)
-    halo_s[...] = ups[512:520].astype(BF16)
-    push(halo_s, halo_r, ha_s, ha_r, z=mod(z + 1, NZ))
-    up(0)
+    push(mine, mine, da_s.at[0], da_r.at[0], c=1 - c)
+
+    def spread_a(e):
+        piece = norm.at[c, y, mod(x - e, NX), :, A]
+        if e:
+            arrive(piece, agx_s.at[e], agx_r.at[e])
+        for d in (2, 1, 3):
+            push(piece, piece, ag2y_s.at[4 * d + e], ag2y_r.at[4 * d + e], y=mod(y + d, NY))
+        if e:
+            push(piece, piece, da_s.at[e], da_r.at[e], c=1 - c)
+
+    def spread_b(e):
+        piece = norm.at[c, mod(y - e, NY), x, :, B]
+        if e:
+            arrive(piece, agy_s.at[e], agy_r.at[e])
+        for d in (2, 1, 3):
+            push(piece, piece, ag2x_s.at[4 * d + e], ag2x_r.at[4 * d + e], x=mod(x + d, NX))
+        if e:
+            push(piece, piece, db_s.at[e], db_r.at[e], c=1 - c)
+
+    spread_a(0)
+    spread_b(0)
+    ring(7, 0)
+    ring(7, 1)
+    for e in (1, 3, 2):
+        spread_a(e)
+        spread_b(e)
+    ring(8, 0)
+    ring(8, 1)
+
+    def collect_a(d):
+        yy = mod(y - d, NY)
+        for e in range(4):
+            arrive(norm.at[c, yy, mod(x - e, NX), :, A], ag2y_s.at[4 * d + e], ag2y_r.at[4 * d + e])
+        piece = norm.at[c, yy, :, :, A]
+        push(piece, piece, da_s.at[3 + d], da_r.at[3 + d], c=1 - c)
+
+    def collect_b(d):
+        xx = mod(x - d, NX)
+        for e in range(4):
+            arrive(norm.at[c, mod(y - e, NY), xx, :, B], ag2x_s.at[4 * d + e], ag2x_r.at[4 * d + e])
+        piece = norm.at[c, :, xx, :, B]
+        push(piece, piece, db_s.at[3 + d], db_r.at[3 + d], c=1 - c)
+
+    def up_a(d):
+        yy = mod(y - d, NY)
+        if d:
+            arrive(norm.at[1 - c, yy, :, :, A], da_s.at[3 + d], da_r.at[3 + d])
+        else:
+            arrive(norm.at[1 - c, y, x], da_s.at[0], da_r.at[0])
+            for e in (1, 3, 2):
+                arrive(norm.at[1 - c, y, mod(x - e, NX), :, A], da_s.at[e], da_r.at[e])
+        rows = norm[:, yy, :, :, 0:HALF].reshape(128, HALF)
+        part = dot(rows, weights[0:8, :, 0:384].reshape(HALF, 384))
+        part = part.reshape(2, 4, 16, 384)
+        acc[:, yy] = acc[:, yy] + part if d == 2 else part
+
+    def up_b(d):
+        xx = mod(x - d, NX)
+        if d:
+            arrive(norm.at[1 - c, :, xx, :, B], db_s.at[3 + d], db_r.at[3 + d])
+        else:
+            for e in (1, 3, 2):
+                arrive(norm.at[1 - c, mod(y - e, NY), x, :, B], db_s.at[e], db_r.at[e])
+        rows = norm[:, :, xx, :, HALF:D].reshape(128, HALF)
+        part = dot(rows, weights[8:16, :, 0:384].reshape(HALF, 384))
+        acc[:, :, xx] = acc[:, :, xx] + part.reshape(2, 4, 16, 384)
+
+    acc[:, mod(y - 2, NY)] = jnp.zeros((2, 4, 16, 384), F32)
+    up_a(0)
+    for d in (1, 3):
+        collect_a(d)
+        collect_b(d)
+        up_a(d)
+    collect_a(2)
+    collect_b(2)
+    up_b(0)
+    up_b(1)
+    up_b(3)
+    up_a(2)
+    up_b(2)
+    for j in (3, 0, 1, 2):
+        for i in range(NX):
+            for cc in range(2):
+                at = 8 + 128 * j + 32 * i + 16 * cc
+                ups[at : at + 16] = acc[cc, j, i].astype(BF16).astype(F32)
+        if j == 3:
+            halo_s[...] = ups[512:520].astype(BF16)
+            push(halo_s, halo_r, ha_s, ha_r, z=mod(z + 1, NZ))
 
     def fed_down(half):
         tap = taps[y]
@@ -351,11 +423,38 @@
             dc_s.at[half], dc_r.at[half], c=1 - c,
         )
 
+    late = []
+
+    def push_if(there, src, dst, ss, rs, **where):
+        copy = pltpu.make_async_remote_copy(
+            src_ref=src, dst_ref=dst, send_sem=ss, recv_sem=rs, device_id=where,
+            device_id_type=MESH,
+        )
+        pl.when(there)(copy.start)
+        late.append((there, copy))
+
+    def arrive_if(there, dst, ss, rs):
+        @pl.when(there)
+        def _():
+            arrive(dst, ss, rs)
+
     def pair_sum(half):
         arrive(downr.at[pl.ds(2 * half, 2)], dc_s.at[half], dc_r.at[half])
         for j in range(2 * half, 2 * half + 2):
             for i in range(NX):
                 rsum[j, i] = (down[c, j, i].astype(F32) + downr[j, i].astype(F32)).astype(BF16)
+            for d in (2, 1, 3):
+                to = mod(x + d, NX)
+                push(
+                    rsum.at[j, to, :, A], p1a.at[d - 1, j], r1a_s.at[4 * d + j],
+                    r1a_r.at[4 * d + j], x=to,
+                )
+            for e in (2, 1, 3, 0):
+                to = mod(x + e, NX)
+                push_if(
+                    y != j, rsum.at[j, to, :, B], p1b.at[y, to], r1b_s.at[4 * j + e],
+                    r1b_r.at[4 * y + e], y=j,
+                )
 
     fed_down(1)
     arrive(halo_r, ha_s, ha_r)
@@ -363,43 +462,50 @@
     fed_down(0)
     pair_sum(1)
     pair_sum(0)
-    for d in range(1, 4):
-        to = mod(x + d, NX)
-        push(rsum.at[:, to, :, A], p1a.at[d - 1], r1a_s.at[d], r1a_r.at[d], x=to)
-        to = mod(y + d, NY)
-        push(rsum.at[to, :, :, B], p1b.at[d - 1], r1b_s.at[d], r1b_r.at[d], y=to)
-    for d in range(1, 4):
-        arrive(p1a.at[d - 1], r1a_s.at[d], r1a_r.at[d])
-    for i in range(4):
-        total = rsum[i, x, :, 0:HALF].astype(F32)
-        for d in range(3):
-            total = total + p1a[d, i].astype(F32)
-        s2a[i] = total.astype(BF16)
-    for d in range(1, 4):
-        to = mod(y + d, NY)
-        push(s2a.at[to], p2a.at[d - 1], r2a_s.at[d], r2a_r.at[d], y=to)
-    for d in range(1, 4):
-        arrive(p1b.at[d - 1], r1b_s.at[d], r1b_r.at[d])
-    for i in range(4):
-        total = rsum[y, i, :, HALF:D].astype(F32)
-        for d in range(3):
-            total = total + p1b[d, i].astype(F32)
-        s2b[i] = total.astype(BF16)
-    for d in range(1, 4):
-        to = mod(x + d, NX)
-        push(s2b.at[to], p2b.at[d - 1], r2b_s.at[d], r2b_r.at[d], x=to)
-    fa = s2a[y].astype(F32)
-    for d in range(1, 4):
-        arrive(p2a.at[d - 1], r2a_s.at[d], r2a_r.at[d])
-        fa = fa + p2a[d - 1].astype(F32)
+    for j, e in ((2, 2), (3, 1), (0, 3), (1, 0)):
+        total = rsum[j, x, :, 0:HALF].astype(F32)
+        for d in range(1, 4):
+            arrive(p1a.at[d - 1, j], r1a_s.at[4 * d + j], r1a_r.at[4 * d + j])
+            total = total + p1a[d - 1, j].astype(F32)
+        s2a[j] = total.astype(BF16)
+        push_if(y != j, s2a.at[j], p2a.at[y], r2a_s.at[j], r2a_r.at[y], y=j)
+        xx = mod(x + e, NX)
+        for i in range(NY):
+            arrive_if(y != i, p1b.at[i, xx], r1b_s.at[4 * i + e], r1b_r.at[4 * i + e])
+        p1b[y, xx] = rsum[y, xx, :, HALF:D]
+        total = p1b[0, xx].astype(F32)
+        for i in range(1, NY):
+            total = total + p1b[i, xx].astype(F32)
+        s2b[xx] = total.astype(BF16)
+        if e:
+            push(s2b.at[xx], p2b.at[e - 1], r2b_s.at[e], r2b_r.at[e], x=xx)
+    for i in range(NY):
+        arrive_if(y != i, p2a.at[i], r2a_s.at[i], r2a_r.at[i])
+    p2a[y] = s2a[y]
+    fa = p2a[0].astype(F32)
+    for i in range(1, NY):
+        fa = fa + p2a[i].astype(F32)
     fb = s2b[x].astype(F32)
     for d in range(1, 4):
         arrive(p2b.at[d - 1], r2b_s.at[d], r2b_r.at[d])
         fb = fb + p2b[d - 1].astype(F32)
     fed = jnp.concatenate([fa, fb], axis=1)
-    out[...] = (residual[...].astype(F32) + rms(fed) * line(gain_post)).astype(BF16)
+    out[...] = rms(fed) * line(gain_post)
     for copy in sent:
         copy.wait_send()
+    for there, copy in late:
+        pl.when(there)(copy.wait_send)
+
+
+INPUTS = 23
+
+
+def entry(*refs):
+    held, refs = refs[:INPUTS], refs[INPUTS:]
+    outs, near, arrived, rest = refs[:2], refs[2 : 2 + INPUTS], refs[2 + INPUTS], refs[3 + INPUTS :]
+    order = (17, 18, 19, 20, 21, 9, 22, 1, 2, 3, 4, 5, 6, 7, 8, 12, 13, 10, 11, 0, 14, 15, 16)
+    loads = {i: pltpu.make_async_copy(held[i], near[i], arrived.at[i]) for i in order}
+    kernel(*near, *outs, *rest, loads)
 
 
 def body(*args):
@@ -415,7 +521,7 @@
     args.append(jnp.asarray(trig))
     vm = pltpu.VMEM
     sem = pltpu.SemaphoreType.DMA
-    scratch = [
+    scratch = [vm(a.shape, a.dtype) for a in args] + [sem((INPUTS,))] + [
         vm((4, 32, 512), BF16),
         vm((NZ, 128, 512), BF16),
         vm((16, 16, 256), BF16),
@@ -438,15 +544,15 @@
         vm((4, 4, 16, D), BF16),
         vm((4, 4, 16, D), BF16),
         vm((3, 4, 16, HALF), BF16),
-        vm((3, 4, 16, HALF), BF16),
+        vm((4, 4, 16, HALF), BF16),
+        vm((4, 16, HALF), BF16),
         vm((4, 16, HALF), BF16),
         vm((4, 16, HALF), BF16),
         vm((3, 16, HALF), BF16),
-        vm((3, 16, HALF), BF16),
-        vm((16, D), BF16),
+        vm((2, 4, 4, 16, 384), F32),
         sem((4,)), sem((4,)),
-        sem((8,)), sem((8,)),
-        sem((7,)), sem((7,)),
+        sem((16,)), sem((16,)),
+        sem((14,)), sem((14,)),
         sem((15,)), sem((15,)),
         sem((4,)), sem((4,)),
         sem((15,)), sem((15,)),
@@ -454,28 +560,29 @@
         sem((4,)), sem((4,)),
         sem((4,)), sem((4,)),
         sem((4,)), sem((4,)),
-        sem((4,)), sem((4,)),
-        sem((4,)), sem((4,)),
-        sem((4,)), sem((4,)),
-        sem((4,)), sem((4,)),
+        sem((16,)), sem((16,)),
+        sem((16,)), sem((16,)),
+        sem((7,)), sem((7,)),
+        sem((7,)), sem((7,)),
         sem, sem,
         sem((2,)), sem((2,)),
-        sem((4,)), sem((4,)),
-        sem((4,)), sem((4,)),
+        sem((16,)), sem((16,)),
+        sem((16,)), sem((16,)),
         sem((4,)), sem((4,)),
         sem((4,)), sem((4,)),
     ]
-    return pl.pallas_call(
-        kernel,
-        out_shape=jax.ShapeDtypeStruct((16, D), BF16),
-        in_specs=[pl.BlockSpec(memory_space=vm)] * len(args),
-        out_specs=pl.BlockSpec(memory_space=vm),
+    resid, branch = pl.pallas_call(
+        entry,
+        out_shape=(jax.ShapeDtypeStruct((16, D), BF16), jax.ShapeDtypeStruct((16, D), F32)),
+        in_specs=[pl.BlockSpec(memory_space=pl.ANY)] * len(args),
+        out_specs=(pl.BlockSpec(memory_space=vm), pl.BlockSpec(memory_space=vm)),
         scratch_shapes=scratch,
         compiler_params=pltpu.CompilerParams(
             collective_id=0, has_side_effects=True, vmem_limit_bytes=60 * 1024 * 1024
         ),
         name="layer",
     )(*args)
+    return (resid.astype(F32) + branch).astype(BF16)
 
 
 def solution(mesh):

time: 85.2 us -> 83.5 us (0.980)
  Pallas kernels: 83.5 us -> 81.8 us
  other arithmetic: 0 us -> 1.55 us
  local copies, waits for them, and re-layouts: 1.47 us -> 0 us
    pallas_call x1, Pallas kernels: 83.5 us -> 81.8 us  [body(): pl.pallas_call(entry, out_shape=(jax.ShapeDtypeStruct((16, D), BF16), jax...]
    convert_element_type x0 -> x1, other arithmetic: none -> 1.55 us  [body(): return (resid.astype(F32) + branch).astype(BF16)]
    unnamed x1 -> x0, local copies, waits for them, and re-layouts: 1.47 us -> none
where the time goes in v3:
time: 83.5 us; the launch traced here: 83.3 us
  Pallas kernels  81.8 us (98%)
  other arithmetic  1.55 us (2%)
    pallas_call x1, Pallas kernels, body(): pl.pallas_call(entry, out_shape=(jax.ShapeDtypeStruct((16, D), BF16), jax...  81.8 us

profile of v3, /device:TPU:1, one launch (start us, length us, event | category | flops | bytes accessed | tf_op | source)
XLA Modules:
  0.0 83.3 jit_solution(1585996303384747973)
XLA Ops:
  0.0 81.8 %layer.1 = (bf16[16,2048]{1,0:T(8,128)(2,1)}, f32[16,2048]{1,0:T(8,128)}) custom-call(bf16[16,2048]{1,0:T(8,128)(2,1)} %refs_0_.1, bf16[128,128]{1,0:T(8,128)(2,1)} %refs_1_.1, bf16[128,128]{1,0:T(8,128)(2,1)} %refs_2_.1, bf16[128,256]{1,0:T(8,128)(2,1)} %refs_3_.1, bf16[64,128]{1,0:T(8,128)(2,1)} %bitcast.2, bf16[64,128]{1,0:T(8,128)(2,1)} %bitcast.3, ...), custom_call_target="tpu_custom_call" | custom-call | tf_op jit(solution)/shard_map/layer/pallas_call | solution.py:574
  81.8 1.6 %add_convert_fusion = bf16[16,2048]{1,0:T(8,128)(2,1)} fusion(f32[16,2048]{1,0:T(8,128)} %get-tuple-element.8, bf16[16,2048]{1,0:T(8,128)(2,1)} %get-tuple-element.7), kind=kLoop, calls=%fused_computation | loop fusion | flops 98304 | bytes 262144 | tf_op jit(solution)/shard_map/convert_element_type | solution.py:585

commit v4 on v3

--- a/solution.py
+++ b/solution.py
@@ -73,7 +73,7 @@
     def greet(**where):
         pl.semaphore_signal(barrier, inc=1, device_id=where, device_id_type=MESH)
 
-    around = [(dz, dy) for dz in range(4) for dy in range(4) if dz or dy]
+    around = [(dz, dy) for dz in (2, 3, 1, 0) for dy in (2, 1, 3, 0) if dz or dy]
 
     def at_group(dz, dy, sign):
         return mod(zl + sign * dz, 4), mod(y + sign * dy, 4)

time: 83.5 us -> 82.9 us (level)
  no operation moved by 1% of the time
where the time goes in v4:
time: 82.9 us; the launch traced here: 82.7 us
  Pallas kernels  81.2 us (98%)
  other arithmetic  1.55 us (2%)
    pallas_call x1, Pallas kernels, body(): pl.pallas_call(entry, out_shape=(jax.ShapeDtypeStruct((16, D), BF16), jax...  81.2 us

profile of v4, /device:TPU:1, one launch (start us, length us, event | category | flops | bytes accessed | tf_op | source)
XLA Modules:
  0.0 82.7 jit_solution(14860276750885189259)
XLA Ops:
  0.0 81.2 %layer.1 = (bf16[16,2048]{1,0:T(8,128)(2,1)}, f32[16,2048]{1,0:T(8,128)}) custom-call(bf16[16,2048]{1,0:T(8,128)(2,1)} %refs_0_.1, bf16[128,128]{1,0:T(8,128)(2,1)} %refs_1_.1, bf16[128,128]{1,0:T(8,128)(2,1)} %refs_2_.1, bf16[128,256]{1,0:T(8,128)(2,1)} %refs_3_.1, bf16[64,128]{1,0:T(8,128)(2,1)} %bitcast.2, bf16[64,128]{1,0:T(8,128)(2,1)} %bitcast.3, ...), custom_call_target="tpu_custom_call" | custom-call | tf_op jit(solution)/shard_map/layer/pallas_call | solution.py:574
  81.2 1.6 %add_convert_fusion = bf16[16,2048]{1,0:T(8,128)(2,1)} fusion(f32[16,2048]{1,0:T(8,128)} %get-tuple-element.8, bf16[16,2048]{1,0:T(8,128)(2,1)} %get-tuple-element.7), kind=kLoop, calls=%fused_computation | loop fusion | flops 98304 | bytes 262144 | tf_op jit(solution)/shard_map/convert_element_type | solution.py:585
